TPU v7x, 32 devices: a whole 2x2x4 slice. The times are simulated.
32 devices in a mesh: kv: 8 (over z, y), tp: 4 (over x, core).
Axes of the slice: x: 2, y: 2, z: 4, core: 2. Of those that a mesh axis runs over, the one named last changes fastest.
Arguments:
- tokens: bfloat16 [64, 4096], P(None, 'kv'), may hold values from -170 to 170
- mix_gain: float32 [4096], P('kv'), may hold values from 0.1 to 1.9
- w_query: bfloat16 [4096, 2048], P('kv', 'tp'), may hold values from -0.09375 to 0.09375
- w_key: bfloat16 [4096, 512], P('kv', 'tp'), may hold values from -0.09375 to 0.09375
- w_value: bfloat16 [4096, 512], P('kv', 'tp'), may hold values from -0.09375 to 0.09375
- w_forget: bfloat16 [4096, 32], P('kv', 'tp'), may hold values from -0.09375 to 0.09375
- query_gain: float32 [64], replicated, may hold values from 0.1 to 1.9
- key_cache: bfloat16 [64, 8, 64, 8192], P(None, 'tp', None, 'kv'), may hold values from -1300 to 1300
- value_cache: bfloat16 [64, 8, 64, 8192], P(None, 'tp', None, 'kv'), may hold values from -8 to 8
- decay_cache: float32 [64, 32, 8192], P(None, 'tp', 'kv'), may hold values from -1066.96 to 0, as said below
- w_out: bfloat16 [2048, 4096], P('tp', 'kv'), may hold values from -1 to 1
- mlp_gain: float32 [4096], P('kv'), may hold values from 0.1 to 1.9
- w_up: bfloat16 [4096, 16384], P('kv', 'tp'), may hold values from -0.09375 to 0.09375
- w_down: bfloat16 [16384, 4096], P('tp', 'kv'), may hold values from -0.046875 to 0.046875
Outputs:
- layer_out: bfloat16 [64, 4096], P(None, 'kv')
Inputs may be any that keep to these rules, and one draw needn't show every extreme that they name: `decay_cache`: each entry is the sum of the non-positive log forget gates of the later cached positions of its sequence and head: 0 at the last cached position, never smaller at a later position.
All inputs are finite; a program needn't handle non-finite values.
Results may differ from a plain program's by a relative error of at most 0.015.
Values may be sent and summed in bfloat16 or wider, within the bound.
A program may use at most 128 MiB of HBM per device.

v0:
```python
import jax
import jax.numpy as jnp
from jax import lax
from jax.sharding import PartitionSpec as P

D = 4096
HEAD_DIM = 64
EPS = 1e-06


def shards(
    tokens,
    mix_gain,
    w_query,
    w_key,
    w_value,
    w_forget,
    query_gain,
    key_cache,
    value_cache,
    decay_cache,
    w_out,
    mlp_gain,
    w_up,
    w_down,
):
    row_count = tokens.shape[0]
    local_heads = w_forget.shape[1]
    local_groups = key_cache.shape[1]
    sharing = local_heads // local_groups
    score_scale = HEAD_DIM ** (-0.5)
    stream = tokens.astype(jnp.float32)
    squares_mix = jnp.sum(stream * stream, axis=1)
    normed_mix = (stream * mix_gain).astype(jnp.bfloat16)
    query_terms = jnp.dot(normed_mix, w_query, preferred_element_type=jnp.float32)
    key_terms = jnp.dot(normed_mix, w_key, preferred_element_type=jnp.float32)
    value_terms = jnp.dot(normed_mix, w_value, preferred_element_type=jnp.float32)
    forget_terms = jnp.dot(normed_mix, w_forget, preferred_element_type=jnp.float32)
    query_raw, key_raw, value_raw, forget_raw, total_mix = lax.psum(
        (query_terms, key_terms, value_terms, forget_terms, squares_mix), "kv"
    )
    scale_mix = lax.rsqrt(total_mix / D + EPS)[:, None]
    heads_raw = (scale_mix * query_raw).reshape(row_count, local_heads, HEAD_DIM)
    inverse = lax.rsqrt(jnp.mean(heads_raw * heads_raw, axis=-1, keepdims=True) + EPS)
    query = (heads_raw * inverse * query_gain).astype(jnp.bfloat16)
    query = query.reshape(row_count, local_groups, sharing, HEAD_DIM)
    key_new = (scale_mix * key_raw).reshape(row_count, local_groups, HEAD_DIM).astype(jnp.bfloat16)
    value_new = (
        (scale_mix * value_raw).reshape(row_count, local_groups, HEAD_DIM).astype(jnp.bfloat16)
    )
    log_forget = jax.nn.log_sigmoid(scale_mix * forget_raw).reshape(
        row_count, local_groups, sharing
    )
    decay = decay_cache.reshape(row_count, local_groups, sharing, -1)
    scores = (
        jnp.einsum("bgjd,bgdp->bgjp", query, key_cache, preferred_element_type=jnp.float32)
        * score_scale
    )
    scores = scores + decay + log_forget[..., None]
    own_score = (
        jnp.einsum("bgjd,bgd->bgj", query, key_new, preferred_element_type=jnp.float32)
        * score_scale
    )
    local_peak = jnp.max(scores, axis=-1)
    peak_score = jnp.maximum(lax.pmax(local_peak, "kv"), own_score)
    weights = jnp.exp(scores - peak_score[..., None])
    partial_values = jnp.einsum(
        "bgjp,bgdp->bgjd",
        weights.astype(jnp.bfloat16),
        value_cache,
        preferred_element_type=jnp.float32,
    )
    mass_sum, summed = lax.psum((jnp.sum(weights, axis=-1), partial_values), "kv")
    own_weight = jnp.exp(own_score - peak_score)
    totals = mass_sum + own_weight
    own_rounded = lax.optimization_barrier(own_weight.astype(jnp.bfloat16)).astype(jnp.float32)
    summed = summed + own_rounded[..., None] * value_new.astype(jnp.float32)[:, :, None, :]
    head_output = summed / totals[..., None]
    attended = head_output.reshape(row_count, local_heads * HEAD_DIM).astype(jnp.bfloat16)
    attn_terms = jnp.dot(attended, w_out, preferred_element_type=jnp.float32)
    attn_out = lax.psum(attn_terms.astype(jnp.bfloat16), "tp")
    attn_rounded = lax.optimization_barrier(attn_out).astype(jnp.float32)
    residual = (stream + attn_rounded).astype(jnp.bfloat16)
    residual_wide = residual.astype(jnp.float32)
    squares_mlp = jnp.sum(residual_wide * residual_wide, axis=1)
    normed_mlp = (residual_wide * mlp_gain).astype(jnp.bfloat16)
    up_terms = jnp.dot(normed_mlp, w_up, preferred_element_type=jnp.float32)
    up_full, total_mlp = lax.psum((up_terms, squares_mlp), "kv")
    scale_mlp = lax.rsqrt(total_mlp / D + EPS)[:, None]
    hidden = jnp.square(jax.nn.relu(scale_mlp * up_full)).astype(jnp.bfloat16)
    down_terms = jnp.dot(hidden, w_down, preferred_element_type=jnp.float32)
    mlp_out = lax.psum(down_terms.astype(jnp.bfloat16), "tp")
    mlp_rounded = lax.optimization_barrier(mlp_out).astype(jnp.float32)
    return (residual_wide + mlp_rounded).astype(jnp.bfloat16)


def solution(mesh):
    in_specs = (
        P(None, "kv"),
        P("kv"),
        P("kv", "tp"),
        P("kv", "tp"),
        P("kv", "tp"),
        P("kv", "tp"),
        P(),
        P(None, "tp", None, "kv"),
        P(None, "tp", None, "kv"),
        P(None, "tp", "kv"),
        P("tp", "kv"),
        P("kv"),
        P("kv", "tp"),
        P("tp", "kv"),
    )
    out_specs = P(None, "kv")
    return jax.shard_map(shards, mesh=mesh, in_specs=in_specs, out_specs=out_specs, check_vma=False)
```

profile of v0, /device:TPU:0, one launch (start us, length us, event | category | flops | bytes accessed | tf_op | source)
XLA Modules:
  0.0 406.1 jit_solution(14472312958995943851)
XLA Ops:
  6.5 1.0 copy-done
  7.6 1.7 fusion.23
  9.4 1.0 fusion.8
  10.3 1.1 fusion.19
  11.4 1.0 fusion.21
  12.4 39.3 %all-reduce.1 = (f32[64]{0:T(128)S(1)}, f32[64,8]{0,1:T(8,128)S(1)}, f32[64,128]{1,0:T(8,128)S(1)}) all-reduce(f32[64]{0:T(128)S(1)} %fusion.8, f32[64,8]{0,1:T(8,128)S(1)} %fusion.21, f32[64,128]{1,0:T(8,128)S(1)} %fusion.19), channel_id=1, replica_groups=mesh['kv'=8,'tp'=4] {'kv'}, use_global_device_ids=true, to_apply=%region_1.0 | all-reduce | flops 8768 | bytes 70144 | tf_op jit(solution)/shard_map/psum | solution.py:39
  51.7 0.1 copy.23
  51.9 2.0 reshape.49
  54.1 0.2 fusion.17
  54.2 29.6 %all-reduce.8.cloned.1.call-done = f32[64,512]{1,0:T(8,128)} async-done(((f32[64,512]{1,0:T(8,128)}), f32[64,512]{1,0:T(8,128)}) %all-reduce.8.cloned.1.call-update) | async-done | bytes 131088 | tf_op jit(solution)/shard_map/psum | solution.py:39
  83.8 1.0 fusion.31
  84.9 0.1 reduce_sum.37
  85.1 0.1 copy.22
  85.3 0.2 reshape.48
  85.5 0.2 multiply_convert_fusion.2
  85.7 9.4 %fusion.32 = (f32[64,2,4]{2,1,0:T(2,128)S(1)}, f32[64,2,4,1024]{3,2,1,0:T(4,128)}) fusion(f32[64,2,4]{2,1,0:T(2,128)S(1)} %copy.23, f32[64,2,4,1024]{3,2,1,0:T(4,128)S(1)} %reshape.49, bf16[64,2,4,64]{3,2,1,0:T(4,128)(2,1)S(1)} %multiply_convert_fusion.2, bf16[64,2,64,1024]{3,2,1,0:T(8,128)(2,1)} %param.21), kind=kOutput, calls=%fused_computation.47 | convolution fusion | flops 69205504 | bytes 21041152 | tf_op jit(solution)/shard_map/bgjd,bgdp->bgjp/dot_general | solution.py:56
  95.1 35.9 %pmax.7 = f32[64,2,4]{2,1,0:T(2,128)S(1)} all-reduce(f32[64,2,4]{2,1,0:T(2,128)S(1)} %get-tuple-element.14), channel_id=1, replica_groups=mesh['kv'=8,'tp'=4] {'kv'}, use_global_device_ids=true, to_apply=%region_6.0 | all-reduce | flops 512 | bytes 4096 | tf_op jit(solution)/shard_map/pmax | solution.py:65
  131.0 0.3 fusion.33
  131.3 2.6 fusion
  133.9 33.9 %all-reduce = (f32[64,2,4]{2,1,0:T(2,128)S(1)}, f32[64,128]{1,0:T(8,128)S(1)}) all-reduce(f32[64,2,4]{2,1,0:T(2,128)S(1)} %fusion, f32[64,128]{1,0:T(8,128)S(1)} %fusion.17), channel_id=1, replica_groups=mesh['kv'=8,'tp'=4] {'kv'}, use_global_device_ids=true, to_apply=%region_11.12 | all-reduce | flops 8704 | bytes 69632 | tf_op jit(solution)/shard_map/psum | solution.py:73
  168.0 9.0 %fusion.2 = f32[64,2,4,64]{3,2,1,0:T(4,128)} fusion(bf16[64,2,64,1024]{3,2,1,0:T(8,128)(2,1)} %param.22, f32[64,2,4,1024]{3,2,1,0:T(4,128)S(1)} %copy-done.1, f32[64,2,4]{2,1,0:T(2,128)S(1)} %multiply_maximum_fusion), kind=kOutput, calls=%fused_computation.6 | convolution fusion | flops 68157440 | bytes 19007488 | tf_op jit(solution)/shard_map/bgjp,bgdp->bgjd/dot_general | solution.py:67
  177.2 69.7 %all-reduce.10.cloned.1.call-done = f32[64,2,4,64]{3,2,1,0:T(4,128)} async-done(((f32[64,2,4,64]{3,2,1,0:T(4,128)}), f32[64,2,4,64]{3,2,1,0:T(4,128)}) %all-reduce.10.cloned.1.call-update) | async-done | bytes 131088 | tf_op jit(solution)/shard_map/psum | solution.py:73
  246.9 1.3 fusion.7
  248.2 0.1 convert_element_type.88
  248.3 0.8 convolution_convert_fusion.1
  249.2 30.8 %all-reduce.12.cloned.1.call-done = bf16[64,512]{1,0:T(8,128)(2,1)} async-done(((bf16[64,512]{1,0:T(8,128)(2,1)}), bf16[64,512]{1,0:T(8,128)(2,1)}) %all-reduce.12.cloned.1.call-update) | async-done | bytes 65552 | tf_op jit(solution)/shard_map/psum | solution.py:81
  280.1 4.1 %fusion.14 = f32[64,4096]{1,0:T(8,128)} fusion(bf16[512,4096]{1,0:T(8,128)(2,1)} %param.26, f32[512]{0:T(512)S(1)} %copy-done.7, bf16[64,512]{1,0:T(8,128)(2,1)S(1)} %copy-done.2, bf16[64,512]{1,0:T(8,128)(2,1)} %all-reduce.12.cloned.1.call-done), kind=kOutput, calls=%fused_computation.26 | convolution fusion | flops 268664832 | bytes 5376000 | tf_op jit(solution)/shard_map/dot_general | solution.py:87
  284.4 21.7 %psum.85 = f32[64]{0:T(128)S(1)} all-reduce(f32[64]{0:T(128)S(1)} %fusion.11), channel_id=1, replica_groups=mesh['kv'=8,'tp'=4] {'kv'}, use_global_device_ids=true, to_apply=%region_14.15 | all-reduce | flops 64 | bytes 512 | tf_op jit(solution)/shard_map/psum | solution.py:88
  306.1 56.6 %all-reduce.14.cloned.1.call-done = f32[64,4096]{1,0:T(8,128)} async-done(((f32[64,4096]{1,0:T(8,128)}), f32[64,4096]{1,0:T(8,128)}) %all-reduce.14.cloned.1.call-update) | async-done | bytes 1048592 | tf_op jit(solution)/shard_map/psum | solution.py:88
  362.8 4.0 convolution_convert_fusion
  366.8 31.3 %all-reduce.16.cloned.1.call-done = bf16[64,512]{1,0:T(8,128)(2,1)} async-done(((bf16[64,512]{1,0:T(8,128)(2,1)}), bf16[64,512]{1,0:T(8,128)(2,1)}) %all-reduce.16.cloned.1.call-update) | async-done | bytes 65552 | tf_op jit(solution)/shard_map/psum | solution.py:92
  398.1 1.5 fusion.13
  (41 shorter events, 1.1 us)
Async XLA Ops:
  6.5 1.0 copy-start
  6.5 77.3 %all-reduce.8.cloned.1.call-start = ((), (), s32[]{:S(2)}) async-start(), calls=%async_computation | async-start | bytes 262144 | tf_op jit(solution)/shard_map/psum | solution.py:39
  9.3 237.6 %all-reduce.10.cloned.1.call-start = ((), (), s32[]{:S(2)}) async-start(), calls=%async_computation.1 | async-start | bytes 524288 | tf_op jit(solution)/shard_map/psum | solution.py:73
  51.9 2.2 copy-start.2
  51.9 2.2 copy-start.5
  51.9 2.2 copy-start.6
  51.9 33.5 %copy-start.8 = (f32[64]{0:T(128)S(1)}, f32[64]{0:T(128)}, u32[]{:S(2)}) copy-start(f32[64]{0:T(128)} %param.20) | copy-start | bytes 772
  95.1 72.8 %copy-start.1 = (f32[64,2,4,1024]{3,2,1,0:T(4,128)S(1)}, f32[64,2,4,1024]{3,2,1,0:T(4,128)}, u32[]{:S(2)}) copy-start(f32[64,2,4,1024]{3,2,1,0:T(4,128)} %get-tuple-element.15) | copy-start | bytes 6291460
  167.9 80.4 %copy-start.4 = (bf16[512,512]{1,0:T(8,128)(2,1)S(1)}, bf16[512,512]{1,0:T(8,128)(2,1)}, u32[]{:S(2)}) copy-start(bf16[512,512]{1,0:T(8,128)(2,1)} %param.24) | copy-start | bytes 1572868
  167.9 112.1 %copy-start.7 = (f32[512]{0:T(512)S(1)}, f32[512]{0:T(512)}, u32[]{:S(2)}) copy-start(f32[512]{0:T(512)} %param.25) | copy-start | bytes 6148
  176.9 103.1 %all-reduce.12.cloned.1.call-start = ((), (), s32[]{:S(2)}) async-start(), calls=%async_computation.2 | async-start | bytes 131072 | tf_op jit(solution)/shard_map/psum | solution.py:81
  249.2 113.6 %all-reduce.14.cloned.1.call-start = ((), (), s32[]{:S(2)}) async-start(), calls=%async_computation.3 | async-start | bytes 2097152 | tf_op jit(solution)/shard_map/psum | solution.py:88
  280.1 4.2 %copy-start.3 = (bf16[64,512]{1,0:T(8,128)(2,1)S(1)}, bf16[64,512]{1,0:T(8,128)(2,1)}, u32[]{:S(2)}) copy-start(bf16[64,512]{1,0:T(8,128)(2,1)} %all-reduce.12.cloned.1.call-done) | copy-start | bytes 196612
  284.2 113.9 %all-reduce.16.cloned.1.call-start = ((), (), s32[]{:S(2)}) async-start(), calls=%async_computation.4 | async-start | bytes 131072 | tf_op jit(solution)/shard_map/psum | solution.py:92
Sparse Core Ops, SparseCore 0:
  10.7 73.1 all-reduce.7
  177.1 69.7 all-reduce.9
  249.3 30.7 all-reduce.11
  284.4 78.3 all-reduce.13
  366.9 31.1 all-reduce.15
where the time goes:
time: 407 us; the launch traced here: 406 us
  waiting for transfers between devices  218 us (54%)
  blocking collectives  131 us (32%)
  matrix products  31.7 us (8%)
  between operations  13.4 us (3%)
  other arithmetic  8.11 us (2%)
    psum x1, waiting for transfers between devices, shards(): lax.psum((jnp.sum(weights, axis=-1), partial_values), 'kv')  69.7 us
    psum x1, waiting for transfers between devices, shards(): up_full, total_mlp = lax.psum((up_terms, squares_mlp), 'kv')  56.6 us
    psum x1, blocking collectives, shards(): lax.psum((query_terms, key_terms, value_terms, forget_terms, squares_mix)...  39.3 us
    pmax x1, blocking collectives, shards(): peak_score = jnp.maximum(lax.pmax(local_peak, 'kv'), own_score)  35.9 us
    psum x1, blocking collectives, shards(): lax.psum((jnp.sum(weights, axis=-1), partial_values), 'kv')  33.9 us
    psum x1, waiting for transfers between devices, shards(): mlp_out = lax.psum(down_terms.astype(jnp.bfloat16), 'tp')  31.3 us
    psum x1, waiting for transfers between devices, shards(): attn_out = lax.psum(attn_terms.astype(jnp.bfloat16), 'tp')  30.8 us
    psum x1, waiting for transfers between devices, shards(): lax.psum((query_terms, key_terms, value_terms, forget_terms, squares_mix)...  29.6 us
  transfers between devices with their start and end apart: 5, of which 5 were waited for; matrix products, arithmetic and copies ran while one was open for 1% of the time, Pallas kernels for 0%

commit v1 on v0

--- a/solution.py
+++ b/solution.py
@@ -6,6 +6,12 @@
 D = 4096
 HEAD_DIM = 64
 EPS = 1e-06
+
+
+def gather_and_add(block, name):
+    blocks = lax.all_gather(block, name, axis=0, tiled=False)
+    summed = blocks.sum(axis=0)
+    return summed
 
 
 def shards(
@@ -89,7 +95,7 @@
     scale_mlp = lax.rsqrt(total_mlp / D + EPS)[:, None]
     hidden = jnp.square(jax.nn.relu(scale_mlp * up_full)).astype(jnp.bfloat16)
     down_terms = jnp.dot(hidden, w_down, preferred_element_type=jnp.float32)
-    mlp_out = lax.psum(down_terms.astype(jnp.bfloat16), "tp")
+    mlp_out = gather_and_add(down_terms.astype(jnp.bfloat16), "tp")
     mlp_rounded = lax.optimization_barrier(mlp_out).astype(jnp.float32)
     return (residual_wide + mlp_rounded).astype(jnp.bfloat16)
 

time: 407 us -> 380 us (0.934)
  waiting for transfers between devices: 218 us -> 187 us
  blocking collectives: 131 us -> 136 us
    psum x1 -> x0, waiting for transfers between devices: 31.3 us -> none  [shards(): mlp_out = lax.psum(down_terms.astype(jnp.bfloat16), 'tp')]
    all_gather x0 -> x1, blocking collectives: none -> 5.78 us  [gather_and_add(): blocks = lax.all_gather(block, name, axis=0, tiled=False)]
  transfers between devices with their start and end apart: 5 -> 4, of which waited for: 5 -> 4; matrix products, arithmetic and copies ran while one was open for 1% -> 2% of each run, Pallas kernels for 0% -> 0%
where the time goes in v1:
time: 380 us; the launch traced here: 379 us
  waiting for transfers between devices  187 us (49%)
  blocking collectives  136 us (36%)
  matrix products  31 us (8%)
  between operations  13.4 us (4%)
  other arithmetic  7.32 us (2%)
  local copies, waits for them, and re-layouts  3.95 us (1%)
    psum x1, waiting for transfers between devices, shards(): lax.psum((jnp.sum(weights, axis=-1), partial_values), 'kv')  69.7 us
    psum x1, waiting for transfers between devices, shards(): up_full, total_mlp = lax.psum((up_terms, squares_mlp), 'kv')  56.7 us
    psum x1, blocking collectives, shards(): lax.psum((query_terms, key_terms, value_terms, forget_terms, squares_mix)...  39.3 us
    pmax x1, blocking collectives, shards(): peak_score = jnp.maximum(lax.pmax(local_peak, 'kv'), own_score)  35.9 us
    psum x1, blocking collectives, shards(): lax.psum((jnp.sum(weights, axis=-1), partial_values), 'kv')  33.9 us
    psum x1, waiting for transfers between devices, shards(): attn_out = lax.psum(attn_terms.astype(jnp.bfloat16), 'tp')  30.8 us
    psum x1, waiting for transfers between devices, shards(): lax.psum((query_terms, key_terms, value_terms, forget_terms, squares_mix)...  29.6 us
    psum x1, blocking collectives, shards(): up_full, total_mlp = lax.psum((up_terms, squares_mlp), 'kv')  21.7 us
  transfers between devices with their start and end apart: 4, of which 4 were waited for; matrix products, arithmetic and copies ran while one was open for 2% of the time, Pallas kernels for 0%

profile of v1, /device:TPU:0, one launch (start us, length us, event | category | flops | bytes accessed | tf_op | source)
XLA Modules:
  0.0 379.2 jit_solution(14858623425260649025)
XLA Ops:
  6.5 1.0 copy-done
  7.6 1.7 fusion.23
  9.4 1.0 fusion.8
  10.3 1.1 fusion.19
  11.4 1.0 fusion.21
  12.4 39.3 %all-reduce.1 = (f32[64]{0:T(128)S(1)}, f32[64,8]{0,1:T(8,128)S(1)}, f32[64,128]{1,0:T(8,128)S(1)}) all-reduce(f32[64]{0:T(128)S(1)} %fusion.8, f32[64,8]{0,1:T(8,128)S(1)} %fusion.21, f32[64,128]{1,0:T(8,128)S(1)} %fusion.19), channel_id=1, replica_groups=mesh['kv'=8,'tp'=4] {'kv'}, use_global_device_ids=true, to_apply=%region_1.0 | all-reduce | flops 8768 | bytes 70144 | tf_op jit(solution)/shard_map/psum | solution.py:45
  51.7 0.1 copy.23
  51.9 2.0 reshape.49
  54.1 0.2 fusion.17
  54.2 29.6 %all-reduce.7.cloned.1.call-done = f32[64,512]{1,0:T(8,128)} async-done(((f32[64,512]{1,0:T(8,128)}), f32[64,512]{1,0:T(8,128)}) %all-reduce.7.cloned.1.call-update) | async-done | bytes 131088 | tf_op jit(solution)/shard_map/psum | solution.py:45
  83.8 1.0 fusion.31
  84.9 0.1 reduce_sum.49
  85.1 0.1 copy.22
  85.3 0.2 reshape.48
  85.5 0.2 multiply_convert_fusion.2
  85.7 9.4 %fusion.32 = (f32[64,2,4]{2,1,0:T(2,128)S(1)}, f32[64,2,4,1024]{3,2,1,0:T(4,128)}) fusion(f32[64,2,4]{2,1,0:T(2,128)S(1)} %copy.23, f32[64,2,4,1024]{3,2,1,0:T(4,128)S(1)} %reshape.49, bf16[64,2,4,64]{3,2,1,0:T(4,128)(2,1)S(1)} %multiply_convert_fusion.2, bf16[64,2,64,1024]{3,2,1,0:T(8,128)(2,1)} %param.21), kind=kOutput, calls=%fused_computation.47 | convolution fusion | flops 69205504 | bytes 21041152 | tf_op jit(solution)/shard_map/bgjd,bgdp->bgjp/dot_general | solution.py:62
  95.1 35.9 %pmax.7 = f32[64,2,4]{2,1,0:T(2,128)S(1)} all-reduce(f32[64,2,4]{2,1,0:T(2,128)S(1)} %get-tuple-element.14), channel_id=1, replica_groups=mesh['kv'=8,'tp'=4] {'kv'}, use_global_device_ids=true, to_apply=%region_6.0 | all-reduce | flops 512 | bytes 4096 | tf_op jit(solution)/shard_map/pmax | solution.py:71
  131.0 0.3 fusion.33
  131.3 2.6 fusion
  133.9 33.9 %all-reduce = (f32[64,2,4]{2,1,0:T(2,128)S(1)}, f32[64,128]{1,0:T(8,128)S(1)}) all-reduce(f32[64,2,4]{2,1,0:T(2,128)S(1)} %fusion, f32[64,128]{1,0:T(8,128)S(1)} %fusion.17), channel_id=1, replica_groups=mesh['kv'=8,'tp'=4] {'kv'}, use_global_device_ids=true, to_apply=%region_11.12 | all-reduce | flops 8704 | bytes 69632 | tf_op jit(solution)/shard_map/psum | solution.py:79
  168.0 9.0 %fusion.2 = f32[64,2,4,64]{3,2,1,0:T(4,128)} fusion(bf16[64,2,64,1024]{3,2,1,0:T(8,128)(2,1)} %param.22, f32[64,2,4,1024]{3,2,1,0:T(4,128)S(1)} %copy-done.1, f32[64,2,4]{2,1,0:T(2,128)S(1)} %multiply_maximum_fusion), kind=kOutput, calls=%fused_computation.6 | convolution fusion | flops 68157440 | bytes 19007488 | tf_op jit(solution)/shard_map/bgjp,bgdp->bgjd/dot_general | solution.py:73
  177.2 69.7 %all-reduce.9.cloned.1.call-done = f32[64,2,4,64]{3,2,1,0:T(4,128)} async-done(((f32[64,2,4,64]{3,2,1,0:T(4,128)}), f32[64,2,4,64]{3,2,1,0:T(4,128)}) %all-reduce.9.cloned.1.call-update) | async-done | bytes 131088 | tf_op jit(solution)/shard_map/psum | solution.py:79
  246.9 1.3 fusion.7
  248.2 0.1 convert_element_type.90
  248.3 0.8 convolution_convert_fusion.1
  249.2 30.8 %all-reduce.11.cloned.1.call-done = bf16[64,512]{1,0:T(8,128)(2,1)} async-done(((bf16[64,512]{1,0:T(8,128)(2,1)}), bf16[64,512]{1,0:T(8,128)(2,1)}) %all-reduce.11.cloned.1.call-update) | async-done | bytes 65552 | tf_op jit(solution)/shard_map/psum | solution.py:87
  280.1 4.1 %fusion.14 = f32[64,4096]{1,0:T(8,128)} fusion(bf16[512,4096]{1,0:T(8,128)(2,1)} %param.26, f32[512]{0:T(512)S(1)} %copy-done.7, bf16[64,512]{1,0:T(8,128)(2,1)S(1)} %copy-done.2, bf16[64,512]{1,0:T(8,128)(2,1)} %all-reduce.11.cloned.1.call-done), kind=kOutput, calls=%fused_computation.26 | convolution fusion | flops 268664832 | bytes 5376000 | tf_op jit(solution)/shard_map/dot_general | solution.py:93
  284.4 21.7 %psum.78 = f32[64]{0:T(128)S(1)} all-reduce(f32[64]{0:T(128)S(1)} %fusion.11), channel_id=1, replica_groups=mesh['kv'=8,'tp'=4] {'kv'}, use_global_device_ids=true, to_apply=%region_14.15 | all-reduce | flops 64 | bytes 512 | tf_op jit(solution)/shard_map/psum | solution.py:94
  306.1 56.7 %all-reduce.13.cloned.1.call-done = f32[64,4096]{1,0:T(8,128)} async-done(((f32[64,4096]{1,0:T(8,128)}), f32[64,4096]{1,0:T(8,128)}) %all-reduce.13.cloned.1.call-update) | async-done | bytes 1048592 | tf_op jit(solution)/shard_map/psum | solution.py:94
  362.7 3.4 convolution_convert_fusion
  366.1 5.8 %all-gather = bf16[256,512]{1,0:T(8,128)(2,1)S(1)} all-gather(bf16[64,512]{1,0:T(8,128)(2,1)S(1)} %convolution_convert_fusion), channel_id=2, replica_groups=mesh['kv'=8,'tp'=4] {'tp'}, dimensions={0}, use_global_device_ids=true | all-gather | bytes 327680 | tf_op jit(solution)/shard_map/all_gather | solution.py:12
  372.0 0.7 fusion.13
  (40 shorter events, 1.1 us)
Async XLA Ops:
  6.5 1.0 copy-start
  6.5 77.3 %all-reduce.7.cloned.1.call-start = ((), (), s32[]{:S(2)}) async-start(), calls=%async_computation | async-start | bytes 262144 | tf_op jit(solution)/shard_map/psum | solution.py:45
  9.3 237.6 %all-reduce.9.cloned.1.call-start = ((), (), s32[]{:S(2)}) async-start(), calls=%async_computation.1 | async-start | bytes 524288 | tf_op jit(solution)/shard_map/psum | solution.py:79
  51.9 2.2 copy-start.2
  51.9 2.2 copy-start.5
  51.9 2.2 copy-start.6
  51.9 33.5 %copy-start.8 = (f32[64]{0:T(128)S(1)}, f32[64]{0:T(128)}, u32[]{:S(2)}) copy-start(f32[64]{0:T(128)} %param.20) | copy-start | bytes 772
  95.1 72.8 %copy-start.1 = (f32[64,2,4,1024]{3,2,1,0:T(4,128)S(1)}, f32[64,2,4,1024]{3,2,1,0:T(4,128)}, u32[]{:S(2)}) copy-start(f32[64,2,4,1024]{3,2,1,0:T(4,128)} %get-tuple-element.15) | copy-start | bytes 6291460
  167.9 80.4 %copy-start.4 = (bf16[512,512]{1,0:T(8,128)(2,1)S(1)}, bf16[512,512]{1,0:T(8,128)(2,1)}, u32[]{:S(2)}) copy-start(bf16[512,512]{1,0:T(8,128)(2,1)} %param.24) | copy-start | bytes 1572868
  167.9 112.1 %copy-start.7 = (f32[512]{0:T(512)S(1)}, f32[512]{0:T(512)}, u32[]{:S(2)}) copy-start(f32[512]{0:T(512)} %param.25) | copy-start | bytes 6148
  176.9 103.1 %all-reduce.11.cloned.1.call-start = ((), (), s32[]{:S(2)}) async-start(), calls=%async_computation.2 | async-start | bytes 131072 | tf_op jit(solution)/shard_map/psum | solution.py:87
  249.2 113.5 %all-reduce.13.cloned.1.call-start = ((), (), s32[]{:S(2)}) async-start(), calls=%async_computation.3 | async-start | bytes 2097152 | tf_op jit(solution)/shard_map/psum | solution.py:94
  280.1 4.2 %copy-start.3 = (bf16[64,512]{1,0:T(8,128)(2,1)S(1)}, bf16[64,512]{1,0:T(8,128)(2,1)}, u32[]{:S(2)}) copy-start(bf16[64,512]{1,0:T(8,128)(2,1)} %all-reduce.11.cloned.1.call-done) | copy-start | bytes 196612
Sparse Core Ops, SparseCore 0:
  10.7 73.1 all-reduce.6
  177.1 69.7 all-reduce.8
  249.3 30.7 all-reduce.10
  284.4 78.3 all-reduce.12
